TPU v7x, 32 devices: a whole 2x2x4 slice. The times are simulated.
32 devices in a mesh: fs: 8 (over z, y), tp: 4 (over x, core).
Axes of the slice: x: 2, y: 2, z: 4, core: 2. Of those that a mesh axis runs over, the one named last changes fastest.
Arguments:
- tokens: bfloat16 [8192, 2048], P('fs'), may hold values from -6 to 6
- norm_gain: float32 [2048], replicated, may hold values from 0.1 to 1.9
- gate_weight: bfloat16 [2048, 4096], P('fs', 'tp'), may hold values from -0.125 to 0.125
- up_weight: bfloat16 [2048, 4096], P('fs', 'tp'), may hold values from -0.125 to 0.125
- down_weight: bfloat16 [4096, 2048], P('tp', 'fs'), may hold values from -2 to 2
- out_gain: float32 [2048], P('tp'), may hold values from 0.1 to 1.9
Outputs:
- result: bfloat16 [8192, 2048], P('fs', 'tp')
All inputs are finite; a program needn't handle non-finite values.
Results may differ from a plain program's by a relative error of at most 0.014.
Values may be sent and summed in bfloat16 or wider, within the bound.
A program may use at most 64 MiB of HBM per device.

v0:
```python
import functools

import jax
import jax.numpy as jnp
from jax import lax
from jax.experimental import pallas as pl
from jax.experimental.pallas import tpu as pltpu
from jax.sharding import PartitionSpec as P

EPSILON = 1e-06
MESH = pl.DeviceIdType.MESH
PIECES = 2
COLUMN_TILE = 256


def ring_layout(n, n_tp):
    ny = max(n_tp // 2, 1)
    if n % ny or (n // ny) % 2:
        ny = 1
    nz, rest = n // ny, max(ny - 1, 1)

    def position(fs):
        z, y = fs // ny, fs % ny
        k = nz - 1 - z
        odd = k % 2
        back = nz + k * rest + (1 - odd) * (y - 1) + odd * (ny - 1 - y)
        return jnp.where(y == 0, z, back)

    def index(pos):
        q = jnp.maximum(pos - nz, 0)
        k, r = q // rest, q % rest
        odd = k % 2
        back = (nz - 1 - k) * ny + (1 - odd) * (1 + r) + odd * (ny - 1 - r)
        return jnp.where(pos < nz, pos * ny, back)

    return position, index


def kernel(
    n, n_tp, tokens_hbm, norm_gain, gate_hbm, up_hbm, down_hbm, out_gain, out_ref,
    tok, normed, gate, up, down, gate_acc, up_acc, hidden, parts, sib, far, own, sq, sq_all,
    local_sem, ring_send, ring_recv, sib_send, sib_recv, far_send, far_recv, sq_send, sq_recv,
):
    half = n // 2
    nx, cuts = n_tp // 2, down.shape[0] // n
    nb = n * cuts // n_tp
    n_tok, d_model = tok.shape
    rows_in = gate.shape[1]
    n_hid, width = down.shape[1], down.shape[2]
    piece = n_tok // PIECES
    position, index = ring_layout(n, n_tp)
    fs, tp = lax.axis_index("fs"), lax.axis_index("tp")
    x, core = tp // 2, tp % 2
    me = position(fs)
    block_of = {}
    for h in range(half + 1):
        block_of[0, h] = index((me + n - h) % n)
        block_of[1, h] = index((me + h) % n)
    target = (block_of[1, 1], block_of[0, 1])
    sibling = x * 2 + 1 - core

    barrier = pltpu.get_barrier_semaphore()
    for fs_id in target:
        pl.semaphore_signal(barrier, inc=1, device_id={"fs": fs_id}, device_id_type=MESH)
    for d in range(1, n_tp):
        pl.semaphore_signal(
            barrier, inc=1, device_id={"tp": (tp + d) % n_tp}, device_id_type=MESH
        )
    loads = [
        pltpu.make_async_copy(tokens_hbm, tok, local_sem.at[0]),
        pltpu.make_async_copy(gate_hbm, gate.at[fs], local_sem.at[1]),
        pltpu.make_async_copy(up_hbm, up.at[fs], local_sem.at[2]),
    ]
    for j in range(cuts):
        cols = pl.ds(j * width, width)
        loads.append(
            pltpu.make_async_copy(
                down_hbm.at[:, cols], down.at[fs * cuts + j], local_sem.at[3 + j]
            )
        )
    for load in loads:
        load.start()
    pl.semaphore_wait(barrier, 2 + n_tp - 1)

    def view(c, b, h, way):
        if c < 2:
            ref = (gate, up)[c]
            if h == half:
                return ref.at[b, pl.ds(way * (rows_in // 2), rows_in // 2)]
            return ref.at[b]
        if h == half:
            return down.at[b * cuts + c - 2, pl.ds(way * (n_hid // 2), n_hid // 2)]
        return down.at[b * cuts + c - 2]

    def ring_copy(c, way, h, b, first=False):
        dst = view(c, b, h, way)
        src = (gate_hbm, up_hbm)[c] if first and c < 2 else dst
        return pltpu.make_async_remote_copy(
            src_ref=src,
            dst_ref=dst,
            send_sem=ring_send.at[way, h - 1, c],
            recv_sem=ring_recv.at[way, h - 1, c],
            device_id={"fs": target[way]},
            device_id_type=MESH,
        )

    sends = []

    def send(c, way, h):
        copy = ring_copy(c, way, h, block_of[way, h - 1], h == 1)
        copy.start()
        sends.append(copy)

    def arrive(c, way, h):
        ring_copy(c, way, h, block_of[way, h]).wait_recv()

    for c in (0, 1):
        for way in (0, 1):
            send(c, way, 1)

    loads[0].wait()
    tile = min(128, n_tok)

    @pl.loop(0, n_tok // tile)
    def _(i):
        rows = pl.ds(pl.multiple_of(i * tile, tile), tile)
        v = tok[rows, :].astype(jnp.float32)
        r = lax.rsqrt(jnp.mean(v * v, axis=1, keepdims=True) + EPSILON)
        out = (v * r * norm_gain[...]).astype(jnp.bfloat16)
        for j in range(n):
            normed[j, rows, :] = out[:, j * rows_in:(j + 1) * rows_in]

    def accumulate(b, mode):
        n_col = gate.shape[2]
        step = min(COLUMN_TILE, n_col)

        @pl.loop(0, n_col // step)
        def _(i):
            cols = pl.ds(pl.multiple_of(i * step, step), step)
            a = normed[b]
            g = jnp.dot(a, gate[b, :, cols], preferred_element_type=jnp.float32)
            u = jnp.dot(a, up[b, :, cols], preferred_element_type=jnp.float32)
            if mode != "first":
                g = g + gate_acc[:, cols]
                u = u + up_acc[:, cols]
            if mode == "last":
                hidden[:, cols] = (g * (1.0 / (1.0 + jnp.exp(-g))) * u).astype(jnp.bfloat16)
            else:
                gate_acc[:, cols] = g
                up_acc[:, cols] = u

    loads[1].wait()
    loads[2].wait()
    accumulate(fs, "first")
    for load in loads[3:]:
        load.wait()

    for h in range(1, half + 1):
        for c in (0, 1):
            for way in (0, 1):
                arrive(c, way, h)
                if h < half:
                    send(c, way, h + 1)
        if h == half - 1:
            for j in range(cuts):
                for way in (0, 1):
                    send(2 + j, way, 1)
        if h < half:
            accumulate(block_of[0, h], "mid")
            accumulate(block_of[1, h], "mid")
        else:
            accumulate(block_of[0, h], "last")

    def owner(b):
        t = b // nb
        return t // 2, t % 2, b % nb

    def piece_rows(q):
        return pl.ds(pl.multiple_of(q * piece, piece), piece)

    def sib_copy(b, slot, q):
        return pltpu.make_async_remote_copy(
            src_ref=parts.at[b, piece_rows(q)],
            dst_ref=sib.at[slot, piece_rows(q)],
            send_sem=sib_send.at[slot, q],
            recv_sem=sib_recv.at[slot, q],
            device_id={"tp": sibling},
            device_id_type=MESH,
        )

    def far_copy(b, x_to, x_from, k, q):
        return pltpu.make_async_remote_copy(
            src_ref=parts.at[b, piece_rows(q)],
            dst_ref=far.at[x_from, k, piece_rows(q)],
            send_sem=far_send.at[x_to * nb + k, q],
            recv_sem=far_recv.at[x_from, k, q],
            device_id={"tp": x_to * 2 + core},
            device_id_type=MESH,
        )

    def multiply(b):
        x_to, core_to, k = owner(b)

        @pl.loop(0, PIECES)
        def _(q):
            rows = piece_rows(q)
            parts[b, rows, :] = jnp.dot(
                hidden[rows, :], down[b], preferred_element_type=jnp.float32
            ).astype(jnp.bfloat16)

            @pl.when(core_to != core)
            def _():
                sib_copy(b, x_to * nb + k, q).start()

    def reduce(b):
        x_to, core_to, k = owner(b)

        @pl.when((core_to == core) & (x_to != x))
        def _():
            @pl.loop(0, PIECES)
            def _(q):
                rows = piece_rows(q)
                slot = x_to * nb + k
                sib_copy(b, slot, q).wait_recv()
                parts[b, rows, :] = (
                    parts[b, rows, :].astype(jnp.float32) + sib[slot, rows, :].astype(jnp.float32)
                ).astype(jnp.bfloat16)
                far_copy(b, x_to, x, k, q).start()

    ready = [fs * cuts + j for j in range(cuts)]
    for h in range(1, half + 1):
        for j in range(cuts):
            for way in (0, 1):
                arrive(2 + j, way, h)
                if h < half:
                    send(2 + j, way, h + 1)
            for way in (0, 1) if h < half else (0,):
                ready.append(block_of[way, h] * cuts + j)
            for b in ready:
                multiply(b)
            for b in ready:
                reduce(b)
            ready = []

    @pl.loop(0, PIECES)
    def _(q):
        rows = piece_rows(q)
        squares = jnp.zeros((piece, 1), jnp.float32)
        for k in range(nb):
            b, slot = tp * nb + k, x * nb + k
            v = parts[b, rows, :].astype(jnp.float32)
            sib_copy(b, slot, q).wait_recv()
            v = v + sib[slot, rows, :].astype(jnp.float32)
            for d in range(1, nx):
                x_from = (x + d) % nx
                far_copy(b, x, x_from, k, q).wait_recv()
                v = v + far[x_from, k, rows, :].astype(jnp.float32)
            own[k, rows, :] = v
            squares = squares + jnp.sum(v * v, axis=1, keepdims=True)
        sq[q] = jnp.transpose(jnp.broadcast_to(squares, (piece, 128)))[0:8, :]

    def sq_copy(to, slot):
        return pltpu.make_async_remote_copy(
            src_ref=sq,
            dst_ref=sq_all.at[slot],
            send_sem=sq_send.at[to],
            recv_sem=sq_recv.at[slot],
            device_id={"tp": to},
            device_id_type=MESH,
        )

    others = [(tp + d) % n_tp for d in range(1, n_tp)]
    for t in others:
        sq_copy(t, tp).start()
    for t in others:
        sq_copy(t, t).wait_recv()

    @pl.loop(0, PIECES)
    def _(q):
        rows = piece_rows(q)
        total = sq[q]
        for t in others:
            total = total + sq_all[t, q]
        r = lax.rsqrt(total / d_model + EPSILON)
        r = jnp.transpose(jnp.broadcast_to(r[0:1, :], (128, piece)))[:, 0:1]
        for k in range(nb):
            cols = slice(k * width, (k + 1) * width)
            out_ref[rows, cols] = (own[k, rows, :] * r * out_gain[:, cols]).astype(jnp.bfloat16)

    for t in others:
        sq_copy(t, tp).wait_send()
    for copy in sends:
        copy.wait_send()

    @pl.loop(0, PIECES)
    def _(q):
        for slot in range(nx * nb):
            sib_copy(slot, slot, q).wait_send()
        for d in range(1, nx):
            for k in range(nb):
                far_copy(k, (x + d) % nx, x, k, q).wait_send()


def body(n, n_tp, tokens, norm_gain, gate_weight, up_weight, down_weight, out_gain):
    n_tok, d_model = tokens.shape
    rows_in, n_hid = gate_weight.shape
    cuts = max(down_weight.shape[1] // 128, 1)
    width = down_weight.shape[1] // cuts
    half, nx, nb = n // 2, n_tp // 2, n * cuts // n_tp
    piece = n_tok // PIECES
    bf16, f32 = jnp.bfloat16, jnp.float32
    dma = pltpu.SemaphoreType.DMA
    hbm = pl.BlockSpec(memory_space=pl.ANY)
    vmem = pl.BlockSpec(memory_space=pltpu.VMEM)
    return pl.pallas_call(
        functools.partial(kernel, n, n_tp),
        out_shape=jax.ShapeDtypeStruct((n_tok, out_gain.shape[0]), bf16),
        in_specs=[hbm, vmem, hbm, hbm, hbm, vmem],
        out_specs=vmem,
        scratch_shapes=[
            pltpu.VMEM((n_tok, d_model), bf16),
            pltpu.VMEM((n, n_tok, rows_in), bf16),
            pltpu.VMEM((n, rows_in, n_hid), bf16),
            pltpu.VMEM((n, rows_in, n_hid), bf16),
            pltpu.VMEM((n * cuts, n_hid, width), bf16),
            pltpu.VMEM((n_tok, n_hid), f32),
            pltpu.VMEM((n_tok, n_hid), f32),
            pltpu.VMEM((n_tok, n_hid), bf16),
            pltpu.VMEM((n * cuts, n_tok, width), bf16),
            pltpu.VMEM((nx * nb, n_tok, width), bf16),
            pltpu.VMEM((nx, nb, n_tok, width), bf16),
            pltpu.VMEM((nb, n_tok, width), f32),
            pltpu.VMEM((PIECES, 8, piece), f32),
            pltpu.VMEM((n_tp, PIECES, 8, piece), f32),
            dma((3 + cuts,)),
            dma((2, half, 2 + cuts)),
            dma((2, half, 2 + cuts)),
            dma((nx * nb, PIECES)),
            dma((nx * nb, PIECES)),
            dma((nx * nb, PIECES)),
            dma((nx, nb, PIECES)),
            dma((n_tp,)),
            dma((n_tp,)),
        ],
        compiler_params=pltpu.CompilerParams(
            collective_id=0, has_side_effects=True, vmem_limit_bytes=62 * 1024 * 1024
        ),
        name="ffn_ring",
    )(tokens, norm_gain[None, :], gate_weight, up_weight, down_weight, out_gain[None, :])


def solution(mesh):
    return jax.shard_map(
        functools.partial(body, mesh.shape["fs"], mesh.shape["tp"]),
        mesh=mesh,
        in_specs=(P("fs", None), P(), P("fs", "tp"), P("fs", "tp"), P("tp", "fs"), P("tp")),
        out_specs=P("fs", "tp"),
        check_vma=False,
    )
```

profile of v0, /device:TPU:0, one launch (start us, length us, event | category | flops | bytes accessed | tf_op | source)
XLA Modules:
  0.0 143.2 jit_solution(4063185658259036058)
XLA Ops:
  0.0 140.9 %ffn_ring.1 = bf16[1024,512]{1,0:T(8,128)(2,1)} custom-call(bf16[1024,2048]{1,0:T(8,128)(2,1)} %tokens_hbm.1, f32[1,2048]{1,0:T(1,128)} %bitcast.2, bf16[256,1024]{1,0:T(8,128)(2,1)} %gate_hbm.1, bf16[256,1024]{1,0:T(8,128)(2,1)} %up_hbm.1, bf16[1024,256]{1,0:T(8,128)(2,1)} %down_hbm.1, f32[1,512]{1,0:T(1,128)} %bitcast.3), custom_call_target="tpu_custom_call" | custom-call | tf_op jit(solution)/shard_map/ffn_ring/pallas_call | solution.py:315
  140.9 2.3 %copy.8 = bf16[1024,512]{1,0:T(8,128)(2,1)} copy(bf16[1024,512]{1,0:T(8,128)(2,1)} %ffn_ring.1) | data formatting | bytes 2097152
where the time goes:
time: 143 us
  Pallas kernels  141 us (99%)
  local copies, waits for them, and re-layouts  2.26 us (2%)
    pallas_call x1, Pallas kernels, body(): pl.pallas_call(functools.partial(kernel, n, n_tp), out_shape=jax.ShapeDty...  141 us

commit v1 on v0

--- a/solution.py
+++ b/solution.py
@@ -11,6 +11,8 @@
 MESH = pl.DeviceIdType.MESH
 PIECES = 2
 COLUMN_TILE = 256
+TOKEN_PIECES = 4
+LAG = 6
 
 
 def ring_layout(n, n_tp):
@@ -349,9 +351,602 @@
     )(tokens, norm_gain[None, :], gate_weight, up_weight, down_weight, out_gain[None, :])
 
 
+def line_order(k, nz):
+    others = [s for s in range(nz) if s != k]
+    return sorted(others, key=lambda s: (abs(s - k), abs(2 * s - nz + 1)))
+
+
+def inward_order(k, nz):
+    out = line_order(k, nz)
+    if k in (0, nz - 1):
+        out[0], out[1] = out[1], out[0]
+    return out
+
+
+def line_kernel(
+    n, n_tp, tokens_hbm, norm_gain, gate_hbm, up_hbm, down_hbm, out_gain, out_ref,
+    tok, normed, gate, up, down, gate_acc, up_acc, hidden, parts, sib, near, far, own, squares, sq, sq_all,
+    local_sem, y_send, y_recv, z_send, z_recv, tok_send, tok_recv,
+    sib_send, sib_recv, near_send, near_recv, far_send, far_recv, sq_send, sq_recv,
+):
+    nz = n // 2
+    cuts = down.shape[0] // n
+    nb = n * cuts // n_tp
+    n_own, d_model = tok.shape
+    rows_in, n_hid = gate.shape[1], gate.shape[2]
+    width = down.shape[2]
+    quarter = n_own // n_tp
+    small = quarter // TOKEN_PIECES
+    half_rows = n_own // PIECES
+    fs, tp = lax.axis_index("fs"), lax.axis_index("tp")
+    z, y = fs // 2, fs % 2
+    x, core = tp // 2, tp % 2
+    fs_y = z * 2 + 1 - y
+    sibling, across = x * 2 + 1 - core, (1 - x) * 2 + core
+    has_next = (z < nz - 1, z > 0)
+    inner = (z > 0) & (z < nz - 1)
+    outer = jnp.logical_not(inner)
+    inward = jnp.where(z < nz // 2, 0, 1)
+
+    barrier = pltpu.get_barrier_semaphore()
+    pl.semaphore_signal(barrier, inc=1, device_id={"fs": fs_y}, device_id_type=MESH)
+    for d in range(1, n_tp):
+        pl.semaphore_signal(
+            barrier, inc=1, device_id={"tp": (tp + d) % n_tp}, device_id_type=MESH
+        )
+    for way in (0, 1):
+
+        @pl.when(has_next[way])
+        def _():
+            to = {"fs": fs + 2 - 4 * way}
+            pl.semaphore_signal(barrier, inc=1, device_id=to, device_id_type=MESH)
+
+    keep = pl.ds(pl.multiple_of(y * n_hid, n_hid), n_hid)
+    give = pl.ds(pl.multiple_of((1 - y) * n_hid, n_hid), n_hid)
+    loads = [
+        pltpu.make_async_copy(tokens_hbm, tok, local_sem.at[0]),
+        pltpu.make_async_copy(gate_hbm.at[:, keep], gate.at[fs], local_sem.at[1]),
+        pltpu.make_async_copy(up_hbm.at[:, keep], up.at[fs], local_sem.at[2]),
+    ]
+    for j in range(cuts):
+        cols = pl.ds(j * width, width)
+        loads.append(
+            pltpu.make_async_copy(
+                down_hbm.at[keep, cols], down.at[fs * cuts + j], local_sem.at[3 + j]
+            )
+        )
+    for load in loads:
+        load.start()
+    pl.semaphore_wait(barrier, n_tp + (z > 0).astype(jnp.int32) + (z < nz - 1).astype(jnp.int32))
+
+    def shard(layer, other):
+        return layer * 2 + (1 - y if other else y)
+
+    def view(p, layer):
+        if p < 4:
+            return (gate, up)[p % 2].at[shard(layer, p // 2)]
+        j = p - 4
+        return down.at[layer * 2 * cuts + j]
+
+    def z_copy(p, way, h, layer, src=None):
+        dst = view(p, layer)
+        return pltpu.make_async_remote_copy(
+            src_ref=dst if src is None else src,
+            dst_ref=dst,
+            send_sem=z_send.at[way, h - 1, p],
+            recv_sem=z_recv.at[way, h - 1, p],
+            device_id={"fs": fs + 2 - 4 * way},
+            device_id_type=MESH,
+        )
+
+    def send_own(p, where=None):
+        src = (gate_hbm, up_hbm)[p].at[:, keep] if p < 2 else None
+        for way in (0, 1):
+
+            @pl.when(has_next[way] if where is None else has_next[way] & where(way))
+            def _():
+                z_copy(p, way, 1, z, src).start()
+
+    order = [line_order(k, nz) for k in range(nz)]
+
+    def pick(values):
+        out = jnp.int32(values[0])
+        for k in range(1, nz):
+            out = jnp.where(z == k, values[k], out)
+        return out
+
+    sources = []
+    for i in range(nz - 1):
+        layer = pick([order[k][i] for k in range(nz)])
+        way = pick([int(order[k][i] > k) for k in range(nz)])
+        h = pick([abs(order[k][i] - k) for k in range(nz)])
+        onward = pick([int(0 < k < nz - 1) for k in range(nz)]) == 1
+        sources.append((layer, way, h, onward))
+
+    def receive(i, p):
+        layer, way, h, onward = sources[i]
+        z_copy(p, way, h, layer).wait_recv()
+
+        @pl.when(onward)
+        def _():
+            z_copy(p, way, h + 1, layer).start()
+
+    def take(j):
+        for i in range(nz - 1):
+            receive(i, 4 + j)
+            if i == 0:
+                send_own(4 + j, lambda way: inward != way)
+
+    def y_copy(p):
+        if p < 2:
+            src, dst = (gate_hbm, up_hbm)[p].at[:, give], (gate, up)[p]
+            src, got = src, (gate, up)[p].at[fs_y]
+            dst = (gate, up)[p].at[fs]
+        elif p < 2 + cuts:
+            j = p - 2
+            src = down_hbm.at[give, pl.ds(j * width, width)]
+            dst = down.at[fs * cuts + j]
+        else:
+            rows = token_rows(y, tp, p - 2 - cuts)
+            src = dst = normed.at[:, rows]
+        return pltpu.make_async_remote_copy(
+            src_ref=src,
+            dst_ref=dst,
+            send_sem=y_send.at[p],
+            recv_sem=y_recv.at[p],
+            device_id={"fs": fs_y},
+            device_id_type=MESH,
+        )
+
+    def token_rows(y_of, t, p):
+        start = y_of * n_own + t * quarter + p * small
+        return pl.ds(pl.multiple_of(start, small), small)
+
+    def token_copy(kind, t, p, to):
+        part = normed.at[:, token_rows(1 - y, t, p)]
+        return pltpu.make_async_remote_copy(
+            src_ref=part,
+            dst_ref=part,
+            send_sem=tok_send.at[kind, p],
+            recv_sem=tok_recv.at[kind, p],
+            device_id={"tp": to},
+            device_id_type=MESH,
+        )
+
+    for p in (0, 1):
+        send_own(p)
+    for p in (0, 1):
+        y_copy(p).start()
+
+    loads[0].wait()
+    tile = min(128, n_own)
+    tiles = n_own // tile
+    own_tiles = quarter // tile
+
+    def normalize(i):
+        rows = pl.ds(pl.multiple_of(i * tile, tile), tile)
+        rows_to = pl.ds(pl.multiple_of(y * n_own + i * tile, tile), tile)
+        v = tok[rows, :].astype(jnp.float32)
+        r = lax.rsqrt(jnp.mean(v * v, axis=1, keepdims=True) + EPSILON)
+        out = (v * r * norm_gain[...]).astype(jnp.bfloat16)
+        for j in range(n):
+            normed[j, rows_to, :] = out[:, j * rows_in:(j + 1) * rows_in]
+
+    @pl.loop(0, own_tiles)
+    def _(i):
+        normalize(tp * own_tiles + i)
+
+    for p in range(TOKEN_PIECES):
+        y_copy(2 + cuts + p).start()
+    for j in range(cuts):
+        y_copy(2 + j).start()
+
+    def accumulate(c, b, y_of, mode="mid"):
+        weight, acc = (gate, up)[c], (gate_acc, up_acc)[c]
+        step = min(COLUMN_TILE, n_hid)
+        n_col = n_hid // step
+
+        def part(half, i):
+            rows = pl.ds(pl.multiple_of(half * n_own, n_own), n_own)
+            cols = pl.ds(pl.multiple_of(i * step, step), step)
+            v = jnp.dot(normed[b, rows, :], weight[b, :, cols], preferred_element_type=jnp.float32)
+            if mode != "first":
+                v = v + acc[rows, cols]
+            if mode == "last":
+                g = gate_acc[rows, cols]
+                hidden[rows, cols] = (g * (1.0 / (1.0 + jnp.exp(-g))) * v).astype(jnp.bfloat16)
+            else:
+                acc[rows, cols] = v
+
+        @pl.loop(0, n_col if y_of is not None else 2 * n_col)
+        def _(i):
+            part(*((y_of, i) if y_of is not None else (i // n_col, i % n_col)))
+
+    def tokens_in(p):
+        y_copy(2 + cuts + p).wait_recv()
+        token_copy(0, tp, p, across).start()
+        token_copy(1, tp, p, sibling).start()
+
+    def tokens_on(p):
+        token_copy(0, across, p, across).wait_recv()
+        token_copy(2, across, p, sibling).start()
+
+    @pl.loop(own_tiles, tiles // 2)
+    def _(i):
+        normalize((tp * own_tiles + i) % tiles)
+
+    y_copy(0).wait_recv()
+    send_own(2)
+
+    @pl.loop(tiles // 2, tiles)
+    def _(i):
+        normalize((tp * own_tiles + i) % tiles)
+
+    for load in loads[1:]:
+        load.wait()
+    y_copy(1).wait_recv()
+    send_own(3)
+    for p in (0, 1):
+        receive(0, p)
+    for c in (0, 1):
+        accumulate(c, fs, y, "first")
+    for p in range(TOKEN_PIECES // 2):
+        tokens_in(p)
+    for c in (0, 1):
+        accumulate(c, fs_y, y)
+    for p in (2, 3):
+        receive(0, p)
+
+    @pl.when(inner)
+    def _():
+        for i in range(1, nz - 2):
+            for p in range(4):
+                receive(i, p)
+
+    for p in range(TOKEN_PIECES // 2, TOKEN_PIECES):
+        tokens_in(p)
+        tokens_on(p - TOKEN_PIECES // 2)
+    for p in (0, 1):
+        accumulate(p, shard(sources[0][0], 0), y)
+    for j in range(cuts):
+        y_copy(2 + j).wait_recv()
+    for j in range(2 * cuts):
+        send_own(4 + j, lambda way: outer)
+    for j in range(2 * cuts):
+        send_own(4 + j, lambda way: inner & (inward == way))
+    for p in range(TOKEN_PIECES // 2, TOKEN_PIECES):
+        tokens_on(p)
+    for p in (0, 1):
+        accumulate(p, shard(sources[0][0], 1), y)
+
+    @pl.when(outer)
+    def _():
+        for i in range(1, nz - 2):
+            for p in range(4):
+                receive(i, p)
+
+    for p in range(TOKEN_PIECES):
+        token_copy(1, sibling, p, sibling).wait_recv()
+        token_copy(2, across + 1 - 2 * core, p, sibling).wait_recv()
+
+    last = nz - 2
+
+    def receive_if(where, p):
+        @pl.when(where)
+        def _():
+            receive(last, p)
+
+    for c in (0, 1):
+        accumulate(c, fs, 1 - y, "first")
+        accumulate(c, fs_y, 1 - y)
+        for p in (0, 1):
+            accumulate(c, shard(sources[0][0], p), 1 - y)
+    receive_if(inner, 0)
+    for i in range(1, nz - 2):
+        for p in (0, 1):
+            accumulate(p, shard(sources[i][0], 0), None)
+    receive_if(inner, 1)
+    for i in range(1, nz - 2):
+        for p in (0, 1):
+            accumulate(p, shard(sources[i][0], 1), None)
+    receive_if(outer, 0)
+    accumulate(0, shard(sources[last][0], 0), None)
+    receive_if(inner, 2)
+    receive_if(outer, 1)
+    accumulate(1, shard(sources[last][0], 0), None)
+    receive_if(inner, 3)
+    receive_if(outer, 2)
+    accumulate(0, shard(sources[last][0], 1), None)
+    receive_if(outer, 3)
+
+    @pl.when(inner)
+    def _():
+        take(0)
+
+    accumulate(1, shard(sources[last][0], 1), None, "last")
+
+    def owner(b):
+        t = b // nb
+        return t // 2, t % 2, b % nb
+
+    def block_rows(q):
+        return pl.ds(pl.multiple_of(q * n_own, n_own), n_own)
+
+    def sib_copy(b, slot, q):
+        return pltpu.make_async_remote_copy(
+            src_ref=parts.at[b, block_rows(q)],
+            dst_ref=sib.at[slot, block_rows(q)],
+            send_sem=sib_send.at[slot, q],
+            recv_sem=sib_recv.at[slot, q],
+            device_id={"tp": sibling},
+            device_id_type=MESH,
+        )
+
+    def near_copy(b, q, slot, to):
+        return pltpu.make_async_remote_copy(
+            src_ref=parts.at[b, block_rows(q)],
+            dst_ref=near.at[slot],
+            send_sem=near_send.at[slot],
+            recv_sem=near_recv.at[slot],
+            device_id=to,
+            device_id_type=MESH,
+        )
+
+    def far_copy(b, q, k, to):
+        return pltpu.make_async_remote_copy(
+            src_ref=parts.at[b, block_rows(q)],
+            dst_ref=far.at[k],
+            send_sem=far_send.at[k],
+            recv_sem=far_recv.at[k],
+            device_id=to,
+            device_id_type=MESH,
+        )
+
+    to_y, to_x = {"fs": fs_y}, {"tp": across}
+
+    def multiply(b):
+        x_to, core_to, k = owner(b)
+
+        @pl.loop(0, 2)
+        def _(q):
+            rows = block_rows(q)
+            parts[b, rows, :] = jnp.dot(
+                hidden[rows, :], down[b], preferred_element_type=jnp.float32
+            ).astype(jnp.bfloat16)
+
+            @pl.when(core_to != core)
+            def _():
+                sib_copy(b, x_to * nb + k, q).start()
+
+    def fold(b, slot, q, extra=None):
+        rows = block_rows(q)
+        sib_copy(b, slot, q).wait_recv()
+        v = parts[b, rows, :].astype(jnp.float32) + sib[slot, rows, :].astype(jnp.float32)
+        if extra is not None:
+            v = v + near[extra].astype(jnp.float32)
+        parts[b, rows, :] = v.astype(jnp.bfloat16)
+
+    def reduce(b, y_first):
+        x_to, core_to, k = owner(b)
+        slot = x_to * nb + k
+        if y_first:
+
+            @pl.when(core_to == core)
+            def _():
+                fold(b, slot, 1 - y)
+                near_copy(b, 1 - y, slot, to_y).start()
+
+        else:
+
+            @pl.when((core_to == core) & (x_to != x))
+            def _():
+                @pl.loop(0, 2)
+                def _(i):
+                    q = jnp.where(i == 0, 1 - y, y)
+                    fold(b, slot, q)
+                    near_copy(b, q, q * nb + k, to_x).start()
+
+    def pass_on(b, y_first):
+        x_to, core_to, k = owner(b)
+        slot = x_to * nb + k
+        if y_first:
+
+            @pl.when((core_to == core) & (x_to != x))
+            def _():
+                near_copy(b, y, slot, to_y).wait_recv()
+                fold(b, slot, y, slot)
+                far_copy(b, y, k, to_x).start()
+
+        else:
+
+            @pl.when((core_to == core) & (x_to == x))
+            def _():
+                q = 1 - y
+                near_copy(b, q, q * nb + k, to_x).wait_recv()
+                fold(b, slot, q, q * nb + k)
+                far_copy(b, q, k, to_y).start()
+
+    final_order = [[k] + inward_order(k, nz) for k in range(nz)]
+    steps = []
+
+    def run(step):
+        m = len(steps)
+        b, kind = step
+        steps.append(step)
+        multiply(b)
+        if m >= 1:
+            reduce(*steps[m - 1])
+        if m >= LAG:
+            pass_on(*steps[m - LAG])
+
+    for j in range(2 * cuts):
+        if j + 1 < 2 * cuts:
+
+            @pl.when(inner)
+            def _():
+                take(j + 1)
+
+        for i in range(nz):
+            layer = pick([final_order[k][i] for k in range(nz)])
+            if i:
+                way = pick([int(final_order[k][i] > k) for k in range(nz)])
+                h = pick([abs(final_order[k][i] - k) for k in range(nz)])
+
+                @pl.when(outer)
+                def _():
+                    z_copy(4 + j, way, h, layer).wait_recv()
+
+            run((layer * 2 * cuts + j, j % 2 == 1))
+    reduce(*steps[-1])
+    for step in steps[-LAG:]:
+        pass_on(*step)
+
+    def piece_rows(q):
+        return pl.ds(pl.multiple_of(q * half_rows, half_rows), half_rows)
+
+    for k in range(nb):
+        slot = (x if k % 2 == 1 else y) * nb + k
+        sib_copy(0, x * nb + k, y).wait_recv()
+        near_copy(0, 0, slot, to_x).wait_recv()
+        far_copy(0, 0, k, to_x).wait_recv()
+
+        @pl.loop(0, n_own // tile)
+        def _(i):
+            rows = pl.ds(pl.multiple_of(i * tile, tile), tile)
+            mine = pl.ds(pl.multiple_of(y * n_own + i * tile, tile), tile)
+            v = parts[tp * nb + k, mine, :].astype(jnp.float32)
+            v = v + sib[x * nb + k, mine, :].astype(jnp.float32)
+            v = v + near[slot, rows, :].astype(jnp.float32)
+            v = v + far[k, rows, :].astype(jnp.float32)
+            own[k, rows, :] = v
+            squares[rows, :] = v * v if k == 0 else squares[rows, :] + v * v
+
+    for q in range(PIECES):
+        total = jnp.sum(squares[piece_rows(q), :], axis=1, keepdims=True)
+        sq[q] = jnp.transpose(jnp.broadcast_to(total, (half_rows, 128)))[0:8, :]
+
+    def sq_copy(to, slot):
+        return pltpu.make_async_remote_copy(
+            src_ref=sq,
+            dst_ref=sq_all.at[slot],
+            send_sem=sq_send.at[to],
+            recv_sem=sq_recv.at[slot],
+            device_id={"tp": to},
+            device_id_type=MESH,
+        )
+
+    others = [(tp + d) % n_tp for d in range(1, n_tp)]
+    for t in others:
+        sq_copy(t, tp).start()
+    for t in others:
+        sq_copy(t, t).wait_recv()
+
+    @pl.loop(0, PIECES)
+    def _(q):
+        rows = piece_rows(q)
+        total = sq[q]
+        for t in others:
+            total = total + sq_all[t, q]
+        r = lax.rsqrt(total / d_model + EPSILON)
+        r = jnp.transpose(jnp.broadcast_to(r[0:1, :], (128, half_rows)))[:, 0:1]
+        for k in range(nb):
+            cols = slice(k * width, (k + 1) * width)
+            out_ref[rows, cols] = (own[k, rows, :] * r * out_gain[:, cols]).astype(jnp.bfloat16)
+
+    for t in others:
+        sq_copy(t, tp).wait_send()
+    for p in range(2 + cuts + TOKEN_PIECES):
+        y_copy(p).wait_send()
+    for p in range(TOKEN_PIECES):
+        token_copy(0, tp, p, across).wait_send()
+        token_copy(1, tp, p, sibling).wait_send()
+        token_copy(2, across, p, sibling).wait_send()
+    for p in range(4 + 2 * cuts):
+        for way in (0, 1):
+
+            @pl.when(has_next[way])
+            def _():
+                z_copy(p, way, 1, z).wait_send()
+
+        for layer, way, h, onward in sources:
+
+            @pl.when(onward)
+            def _():
+                z_copy(p, way, h + 1, layer).wait_send()
+
+    @pl.loop(0, 2)
+    def _(q):
+        for x_to in (0, 1):
+            for k in range(nb):
+                sib_copy(0, x_to * nb + k, q).wait_send()
+
+    for k in range(nb):
+        far_copy(0, 0, k, to_x).wait_send()
+        for q in (0, 1):
+            near_copy(0, 0, q * nb + k, to_x).wait_send()
+
+
+def line_body(n, n_tp, tokens, norm_gain, gate_weight, up_weight, down_weight, out_gain):
+    n_own, d_model = tokens.shape
+    rows_in, n_hid = gate_weight.shape[0], gate_weight.shape[1] // 2
+    cuts = max(down_weight.shape[1] // 128, 1)
+    width = down_weight.shape[1] // cuts
+    nz, nb = n // 2, n * cuts // n_tp
+    n_tok = 2 * n_own
+    bf16, f32 = jnp.bfloat16, jnp.float32
+    dma = pltpu.SemaphoreType.DMA
+    hbm = pl.BlockSpec(memory_space=pl.ANY)
+    vmem = pl.BlockSpec(memory_space=pltpu.VMEM)
+    return pl.pallas_call(
+        functools.partial(line_kernel, n, n_tp),
+        out_shape=jax.ShapeDtypeStruct((n_own, out_gain.shape[0]), bf16),
+        in_specs=[hbm, vmem, hbm, hbm, hbm, vmem],
+        out_specs=vmem,
+        scratch_shapes=[
+            pltpu.VMEM((n_own, d_model), bf16),
+            pltpu.VMEM((n, n_tok, rows_in), bf16),
+            pltpu.VMEM((n, rows_in, n_hid), bf16),
+            pltpu.VMEM((n, rows_in, n_hid), bf16),
+            pltpu.VMEM((n * cuts, n_hid, width), bf16),
+            pltpu.VMEM((n_tok, n_hid), f32),
+            pltpu.VMEM((n_tok, n_hid), f32),
+            pltpu.VMEM((n_tok, n_hid), bf16),
+            pltpu.VMEM((n * cuts, n_tok, width), bf16),
+            pltpu.VMEM((2 * nb, n_tok, width), bf16),
+            pltpu.VMEM((2 * nb, n_own, width), bf16),
+            pltpu.VMEM((nb, n_own, width), bf16),
+            pltpu.VMEM((nb, n_own, width), f32),
+            pltpu.VMEM((n_own, width), f32),
+            pltpu.VMEM((PIECES, 8, n_own // PIECES), f32),
+            pltpu.VMEM((n_tp, PIECES, 8, n_own // PIECES), f32),
+            dma((3 + cuts,)),
+            dma((2 + cuts + TOKEN_PIECES,)),
+            dma((2 + cuts + TOKEN_PIECES,)),
+            dma((2, nz - 1, 4 + 2 * cuts)),
+            dma((2, nz - 1, 4 + 2 * cuts)),
+            dma((3, TOKEN_PIECES)),
+            dma((3, TOKEN_PIECES)),
+            dma((2 * nb, 2)),
+            dma((2 * nb, 2)),
+            dma((2 * nb,)),
+            dma((2 * nb,)),
+            dma((nb,)),
+            dma((nb,)),
+            dma((n_tp,)),
+            dma((n_tp,)),
+        ],
+        compiler_params=pltpu.CompilerParams(
+            collective_id=0, has_side_effects=True, vmem_limit_bytes=62 * 1024 * 1024
+        ),
+        name="ffn_line",
+    )(tokens, norm_gain[None, :], gate_weight, up_weight, down_weight, out_gain[None, :])
+
+
 def solution(mesh):
+    n, n_tp = mesh.shape["fs"], mesh.shape["tp"]
+    paired = n_tp == 4 and n % 2 == 0 and n // 2 > 2
     return jax.shard_map(
-        functools.partial(body, mesh.shape["fs"], mesh.shape["tp"]),
+        functools.partial(line_body if paired else body, n, n_tp),
         mesh=mesh,
         in_specs=(P("fs", None), P(), P("fs", "tp"), P("fs", "tp"), P("tp", "fs"), P("tp")),
         out_specs=P("fs", "tp"),

time: 143 us -> 137 us (0.958)
  Pallas kernels: 141 us -> 135 us
    pallas_call x1, Pallas kernels: 141 us -> 135 us  [line_body(): pl.pallas_call(functools.partial(line_kernel, n, n_tp), out_shape=jax.Sha...]
where the time goes in v1:
time: 137 us
  Pallas kernels  135 us (99%)
  local copies, waits for them, and re-layouts  2.26 us (2%)
    pallas_call x1, Pallas kernels, line_body(): pl.pallas_call(functools.partial(line_kernel, n, n_tp), out_shape=jax.Sha...  135 us

profile of v1, /device:TPU:0, one launch (start us, length us, event | category | flops | bytes accessed | tf_op | source)
XLA Modules:
  0.0 136.9 jit_solution(14388308934116735360)
XLA Ops:
  0.0 134.7 %ffn_line.1 = bf16[1024,512]{1,0:T(8,128)(2,1)} custom-call(bf16[1024,2048]{1,0:T(8,128)(2,1)} %tokens_hbm.1, f32[1,2048]{1,0:T(1,128)} %bitcast.2, bf16[256,1024]{1,0:T(8,128)(2,1)} %gate_hbm.1, bf16[256,1024]{1,0:T(8,128)(2,1)} %up_hbm.1, bf16[1024,256]{1,0:T(8,128)(2,1)} %down_hbm.1, f32[1,512]{1,0:T(1,128)} %bitcast.3), custom_call_target="tpu_custom_call" | custom-call | tf_op jit(solution)/shard_map/ffn_line/pallas_call | solution.py:900
  134.7 2.3 %copy.8 = bf16[1024,512]{1,0:T(8,128)(2,1)} copy(bf16[1024,512]{1,0:T(8,128)(2,1)} %ffn_line.1) | data formatting | bytes 2097152

commit v2 on v1

--- a/solution.py
+++ b/solution.py
@@ -12,7 +12,7 @@
 PIECES = 2
 COLUMN_TILE = 256
 TOKEN_PIECES = 4
-LAG = 6
+LAG = 5
 
 
 def ring_layout(n, n_tp):
@@ -359,15 +359,15 @@
 def inward_order(k, nz):
     out = line_order(k, nz)
     if k in (0, nz - 1):
-        out[0], out[1] = out[1], out[0]
+        out = out[1:] + out[:1]
     return out
 
 
 def line_kernel(
-    n, n_tp, tokens_hbm, norm_gain, gate_hbm, up_hbm, down_hbm, out_gain, out_ref,
-    tok, normed, gate, up, down, gate_acc, up_acc, hidden, parts, sib, near, far, own, squares, sq, sq_all,
+    n, n_tp, tokens_hbm, norm_gain, gate_hbm, up_hbm, down_hbm, out_gain, out_hbm,
+    result, tok, normed, gate, up, down, gate_acc, up_acc, hidden, parts, sib, near, far, own, squares, sq, sq_all,
     local_sem, y_send, y_recv, z_send, z_recv, tok_send, tok_recv,
-    sib_send, sib_recv, near_send, near_recv, far_send, far_recv, sq_send, sq_recv,
+    sib_send, sib_recv, near_send, near_recv, far_send, far_recv, sq_send, sq_recv, out_sem,
 ):
     nz = n // 2
     cuts = down.shape[0] // n
@@ -473,9 +473,9 @@
 
     def take(j):
         for i in range(nz - 1):
-            receive(i, 4 + j)
-            if i == 0:
-                send_own(4 + j, lambda way: inward != way)
+            if i != 1:
+                receive(i, 4 + j)
+        send_own(4 + j, lambda way: inward != way)
 
     def y_copy(p):
         if p < 2:
@@ -636,32 +636,34 @@
         def _():
             receive(last, p)
 
+    for p in range(3):
+        receive_if(inner, p)
+
     for c in (0, 1):
         accumulate(c, fs, 1 - y, "first")
         accumulate(c, fs_y, 1 - y)
         for p in (0, 1):
             accumulate(c, shard(sources[0][0], p), 1 - y)
-    receive_if(inner, 0)
+    receive_if(inner, 3)
     for i in range(1, nz - 2):
         for p in (0, 1):
             accumulate(p, shard(sources[i][0], 0), None)
-    receive_if(inner, 1)
     for i in range(1, nz - 2):
         for p in (0, 1):
             accumulate(p, shard(sources[i][0], 1), None)
+
+    @pl.when(inner)
+    def _():
+        for j in range(2 * cuts):
+            receive(1, 4 + j)
+
     receive_if(outer, 0)
     accumulate(0, shard(sources[last][0], 0), None)
-    receive_if(inner, 2)
     receive_if(outer, 1)
     accumulate(1, shard(sources[last][0], 0), None)
-    receive_if(inner, 3)
     receive_if(outer, 2)
     accumulate(0, shard(sources[last][0], 1), None)
     receive_if(outer, 3)
-
-    @pl.when(inner)
-    def _():
-        take(0)
 
     accumulate(1, shard(sources[last][0], 1), None, "last")
 
@@ -682,22 +684,25 @@
             device_id_type=MESH,
         )
 
-    def near_copy(b, q, slot, to):
-        return pltpu.make_async_remote_copy(
-            src_ref=parts.at[b, block_rows(q)],
-            dst_ref=near.at[slot],
-            send_sem=near_send.at[slot],
-            recv_sem=near_recv.at[slot],
+    def part_rows(q, r):
+        return pl.ds(pl.multiple_of(q * n_own + r * half_rows, half_rows), half_rows)
+
+    def near_copy(b, q, r, slot, to):
+        return pltpu.make_async_remote_copy(
+            src_ref=parts.at[b, part_rows(q, r)],
+            dst_ref=near.at[slot, part_rows(0, r)],
+            send_sem=near_send.at[slot, r],
+            recv_sem=near_recv.at[slot, r],
             device_id=to,
             device_id_type=MESH,
         )
 
-    def far_copy(b, q, k, to):
-        return pltpu.make_async_remote_copy(
-            src_ref=parts.at[b, block_rows(q)],
-            dst_ref=far.at[k],
-            send_sem=far_send.at[k],
-            recv_sem=far_recv.at[k],
+    def far_copy(b, q, r, k, sent, to):
+        return pltpu.make_async_remote_copy(
+            src_ref=parts.at[b, part_rows(q, r)],
+            dst_ref=far.at[k, part_rows(0, r)],
+            send_sem=far_send.at[sent, r],
+            recv_sem=far_recv.at[k, r],
             device_id=to,
             device_id_type=MESH,
         )
@@ -718,97 +723,109 @@
             def _():
                 sib_copy(b, x_to * nb + k, q).start()
 
-    def fold(b, slot, q, extra=None):
-        rows = block_rows(q)
-        sib_copy(b, slot, q).wait_recv()
+    def fold(b, slot, q, r, extra=None):
+        rows = part_rows(q, r)
         v = parts[b, rows, :].astype(jnp.float32) + sib[slot, rows, :].astype(jnp.float32)
         if extra is not None:
-            v = v + near[extra].astype(jnp.float32)
+            v = v + near[extra, part_rows(0, r), :].astype(jnp.float32)
         parts[b, rows, :] = v.astype(jnp.bfloat16)
 
-    def reduce(b, y_first):
+    def starts_on_y(x_to, core_to, k):
+        same = x_to == z // (nz // 2)
+        own_layer = x_to * 2 + core_to == z
+        return (k + x_to + core_to) % 2 == 1
+
+    def near_slot(y_first, x_to, k, q):
+        return jnp.where(y_first, x_to, 2 + q) * nb + k
+
+    def reduce(b):
         x_to, core_to, k = owner(b)
+        y_first = starts_on_y(x_to, core_to, k)
         slot = x_to * nb + k
-        if y_first:
-
-            @pl.when(core_to == core)
+
+        @pl.when((core_to == core) & (y_first | (x_to != x)))
+        def _():
+            q = 1 - y
+            to = {"fs": jnp.where(y_first, fs_y, fs), "tp": jnp.where(y_first, tp, across)}
+            sib_copy(b, slot, q).wait_recv()
+            for r in range(PIECES):
+                fold(b, slot, q, r)
+                near_copy(b, q, r, near_slot(y_first, x_to, k, q), to).start()
+
+            @pl.when(jnp.logical_not(y_first))
             def _():
-                fold(b, slot, 1 - y)
-                near_copy(b, 1 - y, slot, to_y).start()
-
-        else:
-
-            @pl.when((core_to == core) & (x_to != x))
-            def _():
-                @pl.loop(0, 2)
-                def _(i):
-                    q = jnp.where(i == 0, 1 - y, y)
-                    fold(b, slot, q)
-                    near_copy(b, q, q * nb + k, to_x).start()
-
-    def pass_on(b, y_first):
+                sib_copy(b, slot, y).wait_recv()
+                for r in range(PIECES):
+                    fold(b, slot, y, r)
+                    near_copy(b, y, r, near_slot(False, x_to, k, y), to_x).start()
+
+    def pass_on(b):
         x_to, core_to, k = owner(b)
+        y_first = starts_on_y(x_to, core_to, k)
         slot = x_to * nb + k
-        if y_first:
-
-            @pl.when((core_to == core) & (x_to != x))
-            def _():
-                near_copy(b, y, slot, to_y).wait_recv()
-                fold(b, slot, y, slot)
-                far_copy(b, y, k, to_x).start()
-
-        else:
-
-            @pl.when((core_to == core) & (x_to == x))
-            def _():
-                q = 1 - y
-                near_copy(b, q, q * nb + k, to_x).wait_recv()
-                fold(b, slot, q, q * nb + k)
-                far_copy(b, q, k, to_y).start()
+
+        @pl.when((core_to == core) & (y_first == (x_to != x)))
+        def _():
+            q = jnp.where(y_first, y, 1 - y)
+            got = near_slot(y_first, x_to, k, q)
+            to = {"fs": jnp.where(y_first, fs, fs_y), "tp": jnp.where(y_first, across, tp)}
+            sib_copy(b, slot, q).wait_recv()
+            for r in range(PIECES):
+                near_copy(b, q, r, got, to_y).wait_recv()
+                fold(b, slot, q, r, got)
+                far_copy(b, q, r, k, slot, to).start()
 
     final_order = [[k] + inward_order(k, nz) for k in range(nz)]
     steps = []
 
-    def run(step):
+    def run(b):
         m = len(steps)
-        b, kind = step
-        steps.append(step)
+        steps.append(b)
         multiply(b)
         if m >= 1:
-            reduce(*steps[m - 1])
+            reduce(steps[m - 1])
         if m >= LAG:
-            pass_on(*steps[m - LAG])
+            pass_on(steps[m - LAG])
 
     for j in range(2 * cuts):
-        if j + 1 < 2 * cuts:
-
-            @pl.when(inner)
+        run(z * 2 * cuts + j)
+    for j in range(2 * cuts):
+
+        @pl.when(inner)
+        def _():
+            if j == 0:
+                take(0)
+            if j + 1 < 2 * cuts:
+                take(j + 1)
+
+        for i in range(1, nz):
+            layer = pick([final_order[k][i] for k in range(nz)])
+            way = pick([int(final_order[k][i] > k) for k in range(nz)])
+            h = pick([abs(final_order[k][i] - k) for k in range(nz)])
+
+            @pl.when(outer)
             def _():
-                take(j + 1)
-
-        for i in range(nz):
-            layer = pick([final_order[k][i] for k in range(nz)])
-            if i:
-                way = pick([int(final_order[k][i] > k) for k in range(nz)])
-                h = pick([abs(final_order[k][i] - k) for k in range(nz)])
-
-                @pl.when(outer)
-                def _():
-                    z_copy(4 + j, way, h, layer).wait_recv()
-
-            run((layer * 2 * cuts + j, j % 2 == 1))
-    reduce(*steps[-1])
-    for step in steps[-LAG:]:
-        pass_on(*step)
+                z_copy(4 + j, way, h, layer).wait_recv()
+
+            run(layer * 2 * cuts + j)
+    reduce(steps[-1])
+    for b in steps[-LAG:]:
+        pass_on(b)
 
     def piece_rows(q):
         return pl.ds(pl.multiple_of(q * half_rows, half_rows), half_rows)
 
+    def out_copy(q):
+        rows = piece_rows(q)
+        return pltpu.make_async_copy(result.at[rows], out_hbm.at[rows], out_sem.at[q])
+
     for k in range(nb):
-        slot = (x if k % 2 == 1 else y) * nb + k
+        slot = near_slot(starts_on_y(x, core, k), x, k, y)
         sib_copy(0, x * nb + k, y).wait_recv()
-        near_copy(0, 0, slot, to_x).wait_recv()
-        far_copy(0, 0, k, to_x).wait_recv()
+        for r in range(PIECES):
+            near_copy(0, 0, r, slot, to_x).wait_recv()
+        for r in range(PIECES):
+            far_copy(0, 0, r, k, k, to_x).wait_recv()
 
         @pl.loop(0, n_own // tile)
         def _(i):
@@ -838,23 +855,6 @@
     others = [(tp + d) % n_tp for d in range(1, n_tp)]
     for t in others:
         sq_copy(t, tp).start()
-    for t in others:
-        sq_copy(t, t).wait_recv()
-
-    @pl.loop(0, PIECES)
-    def _(q):
-        rows = piece_rows(q)
-        total = sq[q]
-        for t in others:
-            total = total + sq_all[t, q]
-        r = lax.rsqrt(total / d_model + EPSILON)
-        r = jnp.transpose(jnp.broadcast_to(r[0:1, :], (128, half_rows)))[:, 0:1]
-        for k in range(nb):
-            cols = slice(k * width, (k + 1) * width)
-            out_ref[rows, cols] = (own[k, rows, :] * r * out_gain[:, cols]).astype(jnp.bfloat16)
-
-    for t in others:
-        sq_copy(t, tp).wait_send()
     for p in range(2 + cuts + TOKEN_PIECES):
         y_copy(p).wait_send()
     for p in range(TOKEN_PIECES):
@@ -880,10 +880,45 @@
             for k in range(nb):
                 sib_copy(0, x_to * nb + k, q).wait_send()
 
-    for k in range(nb):
-        far_copy(0, 0, k, to_x).wait_send()
-        for q in (0, 1):
-            near_copy(0, 0, q * nb + k, to_x).wait_send()
+    for x_to in (0, 1):
+        for k in range(nb):
+            y_first = starts_on_y(x_to, core, k)
+
+            @pl.when(y_first)
+            def _():
+                for r in range(PIECES):
+                    near_copy(0, 0, r, near_slot(True, x_to, k, 0), to_x).wait_send()
+
+            @pl.when(jnp.logical_not(y_first) & (x_to != x))
+            def _():
+                for q in (0, 1):
+                    for r in range(PIECES):
+                        near_copy(0, 0, r, near_slot(False, x_to, k, q), to_x).wait_send()
+
+            @pl.when(y_first == (x_to != x))
+            def _():
+                for r in range(PIECES):
+                    far_copy(0, 0, r, k, x_to * nb + k, to_x).wait_send()
+
+    for t in others:
+        sq_copy(t, t).wait_recv()
+
+    for q in range(PIECES):
+        rows = piece_rows(q)
+        total = sq[q]
+        for t in others:
+            total = total + sq_all[t, q]
+        r = lax.rsqrt(total / d_model + EPSILON)
+        r = jnp.transpose(jnp.broadcast_to(r[0:1, :], (128, half_rows)))
+        for k in range(nb):
+            cols = slice(k * width, (k + 1) * width)
+            result[rows, cols] = (own[k, rows, :] * r * out_gain[:, cols]).astype(jnp.bfloat16)
+        out_copy(q).start()
+    for q in range(PIECES):
+        out_copy(q).wait()
+
+    for t in others:
+        sq_copy(t, tp).wait_send()
 
 
 def line_body(n, n_tp, tokens, norm_gain, gate_weight, up_weight, down_weight, out_gain):
@@ -901,8 +936,9 @@
         functools.partial(line_kernel, n, n_tp),
         out_shape=jax.ShapeDtypeStruct((n_own, out_gain.shape[0]), bf16),
         in_specs=[hbm, vmem, hbm, hbm, hbm, vmem],
-        out_specs=vmem,
+        out_specs=hbm,
         scratch_shapes=[
+            pltpu.VMEM((n_own, out_gain.shape[0]), bf16),
             pltpu.VMEM((n_own, d_model), bf16),
             pltpu.VMEM((n, n_tok, rows_in), bf16),
             pltpu.VMEM((n, rows_in, n_hid), bf16),
@@ -913,7 +949,7 @@
             pltpu.VMEM((n_tok, n_hid), bf16),
             pltpu.VMEM((n * cuts, n_tok, width), bf16),
             pltpu.VMEM((2 * nb, n_tok, width), bf16),
-            pltpu.VMEM((2 * nb, n_own, width), bf16),
+            pltpu.VMEM((4 * nb, n_own, width), bf16),
             pltpu.VMEM((nb, n_own, width), bf16),
             pltpu.VMEM((nb, n_own, width), f32),
             pltpu.VMEM((n_own, width), f32),
@@ -928,12 +964,13 @@
             dma((3, TOKEN_PIECES)),
             dma((2 * nb, 2)),
             dma((2 * nb, 2)),
-            dma((2 * nb,)),
-            dma((2 * nb,)),
-            dma((nb,)),
-            dma((nb,)),
+            dma((4 * nb, PIECES)),
+            dma((4 * nb, PIECES)),
+            dma((2 * nb, PIECES)),
+            dma((nb, PIECES)),
             dma((n_tp,)),
             dma((n_tp,)),
+            dma((PIECES,)),
         ],
         compiler_params=pltpu.CompilerParams(
             collective_id=0, has_side_effects=True, vmem_limit_bytes=62 * 1024 * 1024

time: 137 us -> 131 us (0.956)
  Pallas kernels: 135 us -> 128 us
    pallas_call x1, Pallas kernels: 135 us -> 128 us  [line_body(): pl.pallas_call(functools.partial(line_kernel, n, n_tp), out_shape=jax.Sha...]
where the time goes in v2:
time: 131 us
  Pallas kernels  128 us (98%)
  local copies, waits for them, and re-layouts  2.26 us (2%)
    pallas_call x1, Pallas kernels, line_body(): pl.pallas_call(functools.partial(line_kernel, n, n_tp), out_shape=jax.Sha...  128 us

profile of v2, /device:TPU:0, one launch (start us, length us, event | category | flops | bytes accessed | tf_op | source)
XLA Modules:
  0.0 130.7 jit_solution(831289795472334613)
XLA Ops:
  0.0 128.4 %ffn_line.1 = bf16[1024,512]{1,0:T(8,128)(2,1)} custom-call(bf16[1024,2048]{1,0:T(8,128)(2,1)} %tokens_hbm.1, f32[1,2048]{1,0:T(1,128)} %bitcast.2, bf16[256,1024]{1,0:T(8,128)(2,1)} %gate_hbm.1, bf16[256,1024]{1,0:T(8,128)(2,1)} %up_hbm.1, bf16[1024,256]{1,0:T(8,128)(2,1)} %down_hbm.1, f32[1,512]{1,0:T(1,128)} %bitcast.3), custom_call_target="tpu_custom_call" | custom-call | tf_op jit(solution)/shard_map/ffn_line/pallas_call | solution.py:935
  128.4 2.3 %copy.8 = bf16[1024,512]{1,0:T(8,128)(2,1)} copy(bf16[1024,512]{1,0:T(8,128)(2,1)} %ffn_line.1) | data formatting | bytes 2097152

commit v3 on v2

--- a/solution.py
+++ b/solution.py
@@ -13,6 +13,7 @@
 COLUMN_TILE = 256
 TOKEN_PIECES = 4
 LAG = 5
+FIRST = 2
 
 
 def ring_layout(n, n_tp):
@@ -733,7 +734,8 @@
     def starts_on_y(x_to, core_to, k):
         same = x_to == z // (nz // 2)
         own_layer = x_to * 2 + core_to == z
-        return (k + x_to + core_to) % 2 == 1
+        odd = (k + x_to + core_to) % 2 == 1
+        return jnp.where(same, odd & (own_layer | (k != nb // 2)), odd | (k == nb - 1))
 
     def near_slot(y_first, x_to, k, q):
         return jnp.where(y_first, x_to, 2 + q) * nb + k
@@ -787,17 +789,25 @@
         if m >= LAG:
             pass_on(steps[m - LAG])
 
+    early = list(range(2 * cuts))
+
+    def run_own(count):
+        for j in early[:count]:
+            run(z * 2 * cuts + j)
+        del early[:count]
+
+    def take_inner(j):
+        if j < 2 * cuts:
+
+            @pl.when(inner)
+            def _():
+                take(j)
+
+    run_own(FIRST)
+    take_inner(0)
     for j in range(2 * cuts):
-        run(z * 2 * cuts + j)
-    for j in range(2 * cuts):
-
-        @pl.when(inner)
-        def _():
-            if j == 0:
-                take(0)
-            if j + 1 < 2 * cuts:
-                take(j + 1)
-
+        if j:
+            take_inner(j + 1)
         for i in range(1, nz):
             layer = pick([final_order[k][i] for k in range(nz)])
             way = pick([int(final_order[k][i] > k) for k in range(nz)])
@@ -808,6 +818,9 @@
                 z_copy(4 + j, way, h, layer).wait_recv()
 
             run(layer * 2 * cuts + j)
+            if j == 0 and i == 1:
+                take_inner(1)
+            run_own(1)
     reduce(steps[-1])
     for b in steps[-LAG:]:
         pass_on(b)

time: 131 us -> 130 us (level)
  no operation moved by 1% of the time
where the time goes in v3:
time: 130 us
  Pallas kernels  128 us (98%)
  local copies, waits for them, and re-layouts  2.26 us (2%)
    pallas_call x1, Pallas kernels, line_body(): pl.pallas_call(functools.partial(line_kernel, n, n_tp), out_shape=jax.Sha...  128 us

profile of v3, /device:TPU:0, one launch (start us, length us, event | category | flops | bytes accessed | tf_op | source)
XLA Modules:
  0.0 129.9 jit_solution(15463706038065436626)
XLA Ops:
  0.0 127.7 %ffn_line.1 = bf16[1024,512]{1,0:T(8,128)(2,1)} custom-call(bf16[1024,2048]{1,0:T(8,128)(2,1)} %tokens_hbm.1, f32[1,2048]{1,0:T(1,128)} %bitcast.2, bf16[256,1024]{1,0:T(8,128)(2,1)} %gate_hbm.1, bf16[256,1024]{1,0:T(8,128)(2,1)} %up_hbm.1, bf16[1024,256]{1,0:T(8,128)(2,1)} %down_hbm.1, f32[1,512]{1,0:T(1,128)} %bitcast.3), custom_call_target="tpu_custom_call" | custom-call | tf_op jit(solution)/shard_map/ffn_line/pallas_call | solution.py:948
  127.7 2.3 %copy.8 = bf16[1024,512]{1,0:T(8,128)(2,1)} copy(bf16[1024,512]{1,0:T(8,128)(2,1)} %ffn_line.1) | data formatting | bytes 2097152
